TPU v7x, 32 devices: a whole 2x2x4 slice. The times are simulated.
32 devices in a mesh: ep: 8 (over z, y), tp: 4 (over x, core).
Axes of the slice: x: 2, y: 2, z: 4, core: 2. Of those that a mesh axis runs over, the one named last changes fastest.
Arguments:
- queries: bfloat16 [2048, 2048], P('ep', 'tp'), may hold values from -150 to 150, as said below
- keys: bfloat16 [2048, 512], P('ep', 'tp'), may hold values from -6 to 6
- values: bfloat16 [2048, 512], P('ep', 'tp'), may hold values from -6 to 6
- cum_gates: float32 [2048, 16], P('ep', 'tp'), may hold values from -2048 to 0, as said below
- out_proj: bfloat16 [2048, 4096], P('tp'), may hold values from -0.125 to 0.125
- tokens: bfloat16 [1024, 4096], P('ep'), may hold values from -6 to 6
- norm_gain: float32 [4096], replicated, may hold values from 0.1 to 1.9
- routes: int32 [1024, 4], P('ep'), may hold values from 0 to 7, all different within a row; in each aligned block of 128 rows (0 to 127, 128 to 255, ...) at most 128 rows name the same one
- route_weights: float32 [1024, 4], P('ep'), may hold values from 0.2 to 1
- w_gate: bfloat16 [8, 4096, 1024], P('ep', None, 'tp'), may hold values from -0.09375 to 0.09375
- w_up: bfloat16 [8, 4096, 1024], P('ep', None, 'tp'), may hold values from -0.09375 to 0.09375
- w_down: bfloat16 [8, 1024, 4096], P('ep', 'tp'), may hold values from -0.1875 to 0.1875
Outputs:
- attn_mixed: bfloat16 [2048, 4096], P(('ep', 'tp'))
- moe_out: bfloat16 [1024, 4096], P('ep', 'tp')
Inputs may be any that keep to these rules, and one draw needn't show every extreme that they name: keys and queries are of order one except where the draw sets a few queries far larger. `cum_gates`: never rises along positions. `routes`: each row names 4 different experts; among the rows of one index of ep no expert is named by more than 128 rows, a bound that some block reaches in some of them.
All inputs are finite; a program needn't handle non-finite values.
Results may differ from a plain program's by a relative error of at most 0.0109.
Values may be sent and summed in bfloat16 or wider, within the bound.
A program may use at most 128 MiB of HBM per device.

v0:
```python
import math

import jax
import jax.numpy as jnp
from jax import lax
from jax.sharding import PartitionSpec as P

HD = 128


SCORE_FLOOR = -1e30


def attend(queries, keys, values, cum_gates, out_proj):
    local_rows = queries.shape[0]
    groups = keys.shape[1] // HD
    group_ratio = cum_gates.shape[1] // groups
    score_scale = HD ** (-0.5)
    first_row = lax.axis_index("ep") * local_rows
    last_row = first_row + local_rows - 1
    query_four = queries.reshape(local_rows, groups, group_ratio, HD)
    query_gate = cum_gates.reshape(local_rows, groups, group_ratio)
    query_pos = first_row + jnp.arange(local_rows, dtype=jnp.int32)
    initial = (
        jnp.full((local_rows, groups, group_ratio), SCORE_FLOOR, jnp.float32),
        jnp.zeros((local_rows, groups, group_ratio), jnp.float32),
        jnp.zeros((local_rows, groups, group_ratio, HD), jnp.float32),
    )
    key_rows = lax.all_gather(keys.astype(jnp.float32), "ep", axis=0, tiled=True).astype(
        jnp.bfloat16
    )
    value_rows = lax.all_gather(values.astype(jnp.float32), "ep", axis=0, tiled=True).astype(
        jnp.bfloat16
    )
    key_gates = lax.all_gather(cum_gates, "ep", axis=0, tiled=True)
    length = key_rows.shape[0]
    block_len = math.gcd(length, 512)

    def advance(block_index, state):
        offset = block_index * block_len

        def accumulate(current):
            maxima, totals, weighted = current
            key_block = lax.dynamic_slice_in_dim(key_rows, offset, block_len, 0).reshape(
                block_len, groups, HD
            )
            value_block = lax.dynamic_slice_in_dim(value_rows, offset, block_len, 0).reshape(
                block_len, groups, HD
            )
            gate_block = lax.dynamic_slice_in_dim(key_gates, offset, block_len, 0).reshape(
                block_len, groups, group_ratio
            )
            scores = (
                jnp.einsum(
                    "qgrd,kgd->qgrk", query_four, key_block, preferred_element_type=jnp.float32
                )
                * score_scale
            )
            scores = scores + query_gate[..., None] - jnp.transpose(gate_block, (1, 2, 0))[None]
            key_pos = offset + jnp.arange(block_len, dtype=jnp.int32)
            allowed = key_pos[None, :] <= query_pos[:, None]
            scores = jnp.where(allowed[:, None, None, :], scores, SCORE_FLOOR)
            new_max = jnp.maximum(maxima, jnp.max(scores, axis=-1))
            factor = jnp.exp(maxima - new_max)
            weights = jnp.exp(scores - new_max[..., None])
            totals = factor * totals + jnp.sum(weights, axis=-1)
            weighted = factor[..., None] * weighted + jnp.einsum(
                "qgrk,kgd->qgrd",
                weights.astype(jnp.bfloat16),
                value_block,
                preferred_element_type=jnp.float32,
            )
            return (new_max, totals, weighted)

        return lax.cond(offset <= last_row, accumulate, lambda kept_state: kept_state, state)

    maxima, totals, weighted = lax.fori_loop(0, length // block_len, advance, initial)
    heads_out = (
        (weighted / totals[..., None])
        .astype(jnp.bfloat16)
        .reshape(local_rows, groups * group_ratio * HD)
    )
    return lax.psum_scatter(
        jnp.dot(heads_out, out_proj, preferred_element_type=jnp.float32).astype(jnp.bfloat16),
        "tp",
        scatter_dimension=0,
        tiled=True,
    )


def experts_part(tokens, norm_gain, routes, route_weights, w_gate, w_up, w_down):
    row_count = tokens.shape[0]
    feature_count = tokens.shape[1]
    top_count = routes.shape[1]
    experts = w_gate.shape[0] * lax.axis_size("ep")
    tp_count = lax.axis_size("tp")
    capacity = 2 * row_count * top_count // experts
    tokens_wide = tokens.astype(jnp.float32)
    normed = (
        tokens_wide
        * lax.rsqrt(jnp.mean(tokens_wide * tokens_wide, axis=-1, keepdims=True) + 1e-06)
        * norm_gain
    ).astype(jnp.bfloat16)
    flat_ids = routes.reshape(-1)
    onehot = (flat_ids[:, None] == jnp.arange(experts, dtype=jnp.int32)[None, :]).astype(jnp.int32)
    slot_rank = jnp.sum((jnp.cumsum(onehot, axis=0) - 1) * onehot, axis=1)
    slot_ids = flat_ids * capacity + slot_rank
    owner_row = jnp.arange(row_count * top_count, dtype=jnp.int32) // top_count
    slot_rows = jnp.full((experts * capacity,), -1, jnp.int32).at[slot_ids].set(owner_row)
    filled = slot_rows >= 0
    outgoing = jnp.where(
        filled[:, None], normed[jnp.maximum(slot_rows, 0)], jnp.zeros((), jnp.bfloat16)
    )
    share_size = capacity // tp_count
    blocks = outgoing.reshape(experts, capacity, feature_count)
    own_part = lax.dynamic_slice_in_dim(blocks, lax.axis_index("tp") * share_size, share_size, 1)
    partial_in = lax.all_to_all(own_part, "ep", split_axis=0, concat_axis=0, tiled=True)
    arrived = lax.all_gather(partial_in, "tp", axis=1, tiled=True).reshape(-1, feature_count)
    gate_act = jnp.dot(arrived, w_gate[0], preferred_element_type=jnp.float32)
    up_act = jnp.dot(arrived, w_up[0], preferred_element_type=jnp.float32)
    latent_width = (jax.nn.silu(gate_act) * up_act).astype(jnp.bfloat16)
    partial_value = jnp.dot(latent_width, w_down[0], preferred_element_type=jnp.float32)
    results = lax.psum_scatter(
        partial_value.astype(jnp.bfloat16), "tp", scatter_dimension=1, tiled=True
    )
    returned_rows = lax.all_to_all(results, "ep", split_axis=0, concat_axis=0, tiled=True)
    picked = returned_rows[slot_ids].astype(jnp.float32).reshape(row_count, top_count, -1)
    return jnp.sum(picked * route_weights[:, :, None], axis=1).astype(jnp.bfloat16)


def per_device(
    queries,
    keys,
    values,
    cum_gates,
    out_proj,
    tokens,
    norm_gain,
    routes,
    route_weights,
    w_gate,
    w_up,
    w_down,
):
    mixed = attend(queries, keys, values, cum_gates, out_proj)
    routed = experts_part(tokens, norm_gain, routes, route_weights, w_gate, w_up, w_down)
    return (mixed, routed)


def solution(mesh):
    placed = (
        P("ep", "tp"),
        P("ep", "tp"),
        P("ep", "tp"),
        P("ep", "tp"),
        P("tp", None),
        P("ep", None),
        P(),
        P("ep", None),
        P("ep", None),
        P("ep", None, "tp"),
        P("ep", None, "tp"),
        P("ep", "tp", None),
    )
    return jax.shard_map(
        per_device,
        mesh=mesh,
        in_specs=placed,
        out_specs=(P(("ep", "tp"), None), P("ep", "tp")),
        check_vma=False,
    )
```

profile of v0, /device:TPU:0, one launch (start us, length us, event | category | flops | bytes accessed | tf_op | source)
XLA Modules:
  0.0 320.0 jit_solution(15044868032597807857)
XLA Ops:
  7.2 0.9 copy.22
  8.4 0.7 broadcast_multiply_fusion
  9.1 1.1 reduce-window.6
  10.2 0.2 slice_reduce_fusion
  10.8 2.4 scatter_custom_fusion
  13.3 1.5 fusion.17
  14.9 1.6 fusion.19
  16.5 7.7 %gather_fusion = bf16[1024,4096]{1,0:T(8,128)(2,1)} fusion(bf16[128,4096]{1,0:T(8,128)(2,1)S(1)} %fusion.19, s32[1024]{0:T(1024)S(1)} %maximum_clamp_fusion), kind=kCustom, calls=%fused_computation | custom fusion | bytes 16781312 | tf_op jit(solution)/shard_map/gather | solution.py:112
  24.2 2.2 dynamic-slice_select_fusion
  26.4 55.4 %all_to_all.17 = bf16[8,32,4096]{2,1,0:T(8,128)(2,1)} all-to-all(bf16[8,32,4096]{2,1,0:T(8,128)(2,1)S(1)} %dynamic-slice_select_fusion), channel_id=1, replica_groups=mesh['ep'=8,'tp'=4] {'ep'}, dimensions={0} | all-to-all | bytes 4194304 | tf_op jit(solution)/shard_map/all_to_all | solution.py:117
  81.9 57.4 %all-gather.2.cloned.1.call-done = bf16[8,128,4096]{2,1,0:T(8,128)(2,1)} async-done(((bf16[8,32,4096]{2,1,0:T(8,128)(2,1)}), bf16[8,128,4096]{2,1,0:T(8,128)(2,1)}) %all-gather.2.cloned.1.call-update) | async-done | bytes 8388624 | tf_op jit(solution)/shard_map/all_gather | solution.py:118
  139.3 6.5 %fusion.23 = f32[1024,256]{1,0:T(8,128)S(1)} fusion(bf16[1024,4096]{1,0:T(8,128)(2,1)} %bitcast.89, bf16[1,4096,256]{2,1,0:T(8,128)(2,1)} %param.25), kind=kOutput, calls=%fused_computation.40 | convolution fusion | flops 2147483648 | bytes 11534336 | tf_op jit(solution)/shard_map/dot_general | solution.py:119
  145.7 0.5 copy-done.7
  146.2 2.4 fusion.28
  148.6 5.6 %convolution_convert_fusion = bf16[1024,4096]{1,0:T(8,128)(2,1)} fusion(bf16[1024,256]{1,0:T(8,128)(2,1)S(1)} %fusion.28, bf16[1,256,4096]{2,1,0:T(8,128)(2,1)S(1)} %copy-done), kind=kOutput, calls=%fused_computation.29 | convolution fusion | flops 2151677952 | bytes 11010048 | tf_op jit(solution)/shard_map/dot_general | solution.py:122
  154.3 0.8 copy-done.3
  155.3 0.2 copy.20
  155.5 30.7 %all_gather.13 = f32[2048,4]{0,1:T(4,128)S(1)} all-gather(f32[256,4]{0,1:T(4,128)S(1)} %copy-done.4), channel_id=1, replica_groups=mesh['ep'=8,'tp'=4] {'ep'}, dimensions={0}, use_global_device_ids=true | all-gather | bytes 36864 | tf_op jit(solution)/shard_map/all_gather | solution.py:35
  186.2 31.6 %all_gather.14 = bf16[2048,128]{0,1:T(8,128)(2,1)S(1)} all-gather(bf16[256,128]{0,1:T(8,128)(2,1)S(1)} %copy.19), channel_id=1, replica_groups=mesh['ep'=8,'tp'=4] {'ep'}, dimensions={0}, use_global_device_ids=true | all-gather | bytes 589824 | tf_op jit(solution)/shard_map/all_gather | solution.py:32
  217.8 33.4 %all_gather.12 = bf16[2048,128]{1,0:T(8,128)(2,1)} all-gather(bf16[256,128]{1,0:T(8,128)(2,1)S(1)} %copy-done.2), channel_id=1, replica_groups=mesh['ep'=8,'tp'=4] {'ep'}, dimensions={0}, use_global_device_ids=true | all-gather | bytes 589824 | tf_op jit(solution)/shard_map/all_gather | solution.py:29
  251.2 2.9 while.18
  251.3 2.7 conditional.3
  251.3 0.1 broadcast_compare_fusion
  251.5 1.5 fusion.38
  253.0 0.6 fusion.5
  253.7 0.3 fusion.4
  254.2 4.8 %convolution_convert_fusion.1 = bf16[256,4096]{1,0:T(8,128)(2,1)} fusion(bf16[256,512]{0,1:T(8,128)(2,1)S(1)} %bitcast.83, bf16[512,4096]{1,0:T(8,128)(2,1)} %param.20), kind=kOutput, calls=%fused_computation.30 | convolution fusion | flops 1074790400 | bytes 6553600 | tf_op jit(solution)/shard_map/dot_general | solution.py:84
  259.0 13.7 %all-to-all-start.1 = ((bf16[8,128,1024]{2,1,0:T(8,128)(2,1)}), bf16[8,128,1024]{2,1,0:T(8,128)(2,1)}, u32[]{:S(2)}, u32[]{:S(2)}) async-start(bf16[8,128,1024]{2,1,0:T(8,128)(2,1)} %bitcast.82), calls=%async_computation.3 | async-start | bytes 4194304 | tf_op jit(solution)/shard_map/all_to_all | solution.py:126
  272.9 30.5 %all-to-all-done.1 = bf16[8,128,1024]{2,1,0:T(8,128)(2,1)} async-done(((bf16[8,128,1024]{2,1,0:T(8,128)(2,1)}), bf16[8,128,1024]{2,1,0:T(8,128)(2,1)}, u32[]{:S(2)}, u32[]{:S(2)}) %all-to-all-start.1) | async-done | bytes 2097184 | tf_op jit(solution)/shard_map/all_to_all | solution.py:126
  303.4 4.6 %gather_fusion.1 = bf16[512,1024]{1,0:T(8,128)(2,1)S(1)} fusion(bf16[1024,1024]{1,0:T(8,128)(2,1)} %bitcast.29, s32[1024]{0:T(1024)S(1)} %pad_clamp_fusion), kind=kCustom, calls=%fused_computation.1 | custom fusion | bytes 2099200 | tf_op jit(solution)/shard_map/gather | solution.py:127
  308.0 1.7 reshape.154
  309.7 3.7 %multiply_reduce_fusion = bf16[128,1024]{1,0:T(8,128)(2,1)} fusion(f32[128,4,1024]{2,1,0:T(4,128)} %reshape.154, f32[128,4]{1,0:T(8,128)S(1)} %copy.24), kind=kLoop, calls=%fused_computation.42 | loop fusion | flops 917504 | bytes 2361344 | tf_op jit(solution)/shard_map/reduce_sum | solution.py:128
  (57 shorter events, 1.5 us)
Async XLA Ops:
  7.2 141.4 %copy-start = (bf16[1,256,4096]{2,1,0:T(8,128)(2,1)S(1)}, bf16[1,256,4096]{2,1,0:T(8,128)(2,1)}, u32[]{:S(2)}) copy-start(bf16[1,256,4096]{2,1,0:T(8,128)(2,1)} %param.27) | copy-start | bytes 6291460
  7.2 132.1 %all-gather.2.cloned.1.call-start = ((), (), s32[]{:S(2)}) async-start(), calls=%async_computation.5 | async-start | bytes 10485760 | tf_op jit(solution)/shard_map/all_gather | solution.py:118
  81.8 177.2 %reduce-scatter.5.cloned.1.call-start = ((), (), s32[]{:S(2)}) async-start(), calls=%async_computation.6 | async-start | bytes 10485760 | tf_op jit(solution)/shard_map/reduce_scatter | solution.py:123
  139.3 6.5 %copy-start.6 = (bf16[8,128,4096]{2,1,0:T(8,128)(2,1)S(1)}, bf16[8,128,4096]{2,1,0:T(8,128)(2,1)}, u32[]{:S(2)}) copy-start(bf16[8,128,4096]{2,1,0:T(8,128)(2,1)} %all-gather.2.cloned.1.call-done) | copy-start | bytes 25165828
  139.3 7.0 %copy-start.7 = (bf16[1,4096,256]{2,1,0:T(8,128)(2,1)S(1)}, bf16[1,4096,256]{2,1,0:T(8,128)(2,1)}, u32[]{:S(2)}) copy-start(bf16[1,4096,256]{2,1,0:T(8,128)(2,1)} %param.26) | copy-start | bytes 6291460
  154.2 0.8 copy-start.3
  154.2 1.0 copy-start.1
  154.2 1.3 copy-start.4
  154.2 63.6 %copy-start.2 = (bf16[256,128]{1,0:T(8,128)(2,1)S(1)}, bf16[256,128]{1,0:T(8,128)(2,1)}, u32[]{:S(2)}) copy-start(bf16[256,128]{1,0:T(8,128)(2,1)} %param.17) | copy-start | bytes 196612
  154.2 159.2 %reduce-scatter.3.cloned.1.call-start = ((), (), s32[]{:S(2)}) async-start(), calls=%async_computation.4 | async-start | bytes 2621440 | tf_op jit(solution)/shard_map/reduce_scatter | solution.py:83
  259.0 13.7 %copy-start.5 = (f32[128,4]{0,1:T(4,128)S(1)}, f32[128,4]{0,1:T(4,128)}, u32[]{:S(2)}) copy-start(f32[128,4]{0,1:T(4,128)} %param.24) | copy-start | bytes 6148
  259.0 44.4 %all-to-all-start.1 = ((bf16[8,128,1024]{2,1,0:T(8,128)(2,1)}), bf16[8,128,1024]{2,1,0:T(8,128)(2,1)}, u32[]{:S(2)}, u32[]{:S(2)}) async-start(bf16[8,128,1024]{2,1,0:T(8,128)(2,1)} %bitcast.82), calls=%async_computation.3 | async-start | bytes 4194304 | tf_op jit(solution)/shard_map/all_to_all | solution.py:126
Sparse Core Ops, SparseCore 0:
  82.0 57.2 all-gather.1
  154.3 71.2 reduce-scatter.4
  259.1 39.3 reduce-scatter.2
where the time goes:
time: 320 us
  blocking collectives  151 us (47%)
  waiting for transfers between devices  88 us (28%)
  matrix products  21.3 us (7%)
  local copies, waits for them, and re-layouts  20 us (6%)
  between operations  14 us (4%)
  starting transfers between devices  13.8 us (4%)
  other arithmetic  11.5 us (4%)
    all_gather x1, waiting for transfers between devices, experts_part(): lax.all_gather(partial_in, 'tp', axis=1, tiled=True)  57.4 us
    all_to_all x1, blocking collectives, experts_part(): lax.all_to_all(own_part, 'ep', split_axis=0, concat_axis=0, tiled=True)  55.4 us
    all_gather x1, blocking collectives, attend(): lax.all_gather(keys.astype(jnp.float32), 'ep', axis=0, tiled=True)  33.4 us
    all_gather x1, blocking collectives, attend(): lax.all_gather(values.astype(jnp.float32), 'ep', axis=0, tiled=True)  31.6 us
    all_gather x1, blocking collectives, attend(): key_gates = lax.all_gather(cum_gates, 'ep', axis=0, tiled=True)  30.7 us
    all_to_all x1, waiting for transfers between devices, experts_part(): lax.all_to_all(results, 'ep', split_axis=0, concat_axis=0, tiled=True)  30.5 us
    all_to_all x1, starting transfers between devices, experts_part(): lax.all_to_all(results, 'ep', split_axis=0, concat_axis=0, tiled=True)  13.7 us
    gather x1, local copies, waits for them, and re-layouts, experts_part(): normed[jnp.maximum(slot_rows, 0)]  7.74 us
  transfers between devices with their start and end apart: 4, of which 2 were waited for; matrix products, arithmetic and copies ran while one was open for 6% of the time, Pallas kernels for 0%

commit v1 on v0

--- a/solution.py
+++ b/solution.py
@@ -11,9 +11,43 @@
 SCORE_FLOOR = -1e30
 
 
-def attend(queries, keys, values, cum_gates, out_proj):
+def split_three(x):
+    high = lax.reduce_precision(x, 8, 7)
+    rest = x - high
+    middle = lax.reduce_precision(rest, 8, 7)
+    low = rest - middle
+    return jnp.stack([high, middle, low]).astype(jnp.bfloat16)
+
+
+def join_three(pieces, axis):
+    wide = pieces.astype(jnp.float32)
+    parts = [lax.index_in_dim(wide, i, axis, keepdims=False) for i in range(3)]
+    return (parts[2] + parts[1]) + parts[0]
+
+
+def gather_packed(arrays, axis):
+    lanes = 128
+    rows = []
+    for array in arrays:
+        flat = array.reshape(-1)
+        flat = jnp.pad(flat, (0, -flat.shape[0] % (16 * lanes)))
+        rows.append(flat.reshape(-1, lanes))
+    gathered = lax.all_gather(jnp.concatenate(rows, axis=0), axis, axis=0, tiled=False)
+    count = gathered.shape[0]
+    results = []
+    first = 0
+    for array, block in zip(arrays, rows):
+        piece = gathered[:, first : first + block.shape[0]]
+        if array.size != block.size:
+            piece = piece.reshape(count, -1)[:, : array.size]
+        results.append(piece.reshape((count,) + array.shape))
+        first += block.shape[0]
+    return results
+
+
+def attend(queries, key_rows, value_rows, key_gates, cum_gates, out_proj):
     local_rows = queries.shape[0]
-    groups = keys.shape[1] // HD
+    groups = key_rows.shape[1] // HD
     group_ratio = cum_gates.shape[1] // groups
     score_scale = HD ** (-0.5)
     first_row = lax.axis_index("ep") * local_rows
@@ -26,13 +60,6 @@
         jnp.zeros((local_rows, groups, group_ratio), jnp.float32),
         jnp.zeros((local_rows, groups, group_ratio, HD), jnp.float32),
     )
-    key_rows = lax.all_gather(keys.astype(jnp.float32), "ep", axis=0, tiled=True).astype(
-        jnp.bfloat16
-    )
-    value_rows = lax.all_gather(values.astype(jnp.float32), "ep", axis=0, tiled=True).astype(
-        jnp.bfloat16
-    )
-    key_gates = lax.all_gather(cum_gates, "ep", axis=0, tiled=True)
     length = key_rows.shape[0]
     block_len = math.gcd(length, 512)
 
@@ -128,6 +155,48 @@
     return jnp.sum(picked * route_weights[:, :, None], axis=1).astype(jnp.bfloat16)
 
 
+def normalize(tokens, norm_gain):
+    tokens_wide = tokens.astype(jnp.float32)
+    return (
+        tokens_wide
+        * lax.rsqrt(jnp.mean(tokens_wide * tokens_wide, axis=-1, keepdims=True) + 1e-06)
+        * norm_gain
+    ).astype(jnp.bfloat16)
+
+
+def combine_table(routes, route_weights, experts):
+    chosen = routes[:, :, None] == jnp.arange(experts, dtype=jnp.int32)[None, None, :]
+    return jnp.sum(jnp.where(chosen, route_weights[:, :, None], 0.0), axis=1)
+
+
+def exchange_down(w_down):
+    count = lax.axis_size("tp")
+    me = lax.axis_index("tp")
+    hidden, features = w_down.shape
+    width = features // count
+    result = jnp.zeros((count * hidden, width), w_down.dtype)
+    for offset in range(count):
+        target = (me + offset) % count
+        block = lax.dynamic_slice_in_dim(w_down, target * width, width, 1)
+        if offset:
+            block = lax.ppermute(block, "tp", [(i, (i + offset) % count) for i in range(count)])
+        source = (me - offset) % count
+        result = lax.dynamic_update_slice_in_dim(result, block, source * hidden, 0)
+    return result
+
+
+def experts_dense(rows, table, w_gate, w_up, down):
+    gate_act = jnp.dot(rows, w_gate[0], preferred_element_type=jnp.float32)
+    up_act = jnp.dot(rows, w_up[0], preferred_element_type=jnp.float32)
+    hidden = (jax.nn.silu(gate_act) * up_act).astype(jnp.bfloat16)
+    full = lax.all_gather(hidden, "tp", axis=1, tiled=True)
+    expert_out = jnp.dot(full, down, preferred_element_type=jnp.float32)
+    mine = lax.dynamic_index_in_dim(table, lax.axis_index("ep"), 1, keepdims=True)
+    return lax.psum_scatter(
+        (expert_out * mine).astype(jnp.bfloat16), "ep", scatter_dimension=0, tiled=True
+    )
+
+
 def per_device(
     queries,
     keys,
@@ -142,8 +211,27 @@
     w_up,
     w_down,
 ):
-    mixed = attend(queries, keys, values, cum_gates, out_proj)
-    routed = experts_part(tokens, norm_gain, routes, route_weights, w_gate, w_up, w_down)
+    experts = w_gate.shape[0] * lax.axis_size("ep")
+    row_count, top_count = routes.shape
+    dense = 2 * row_count * top_count // experts >= row_count
+    packed = [keys, values, split_three(cum_gates)]
+    if dense:
+        packed.append(split_three(combine_table(routes, route_weights, experts)))
+    gathered = gather_packed(packed, "ep")
+    key_rows = gathered[0].reshape(-1, keys.shape[1])
+    value_rows = gathered[1].reshape(-1, values.shape[1])
+    key_gates = join_three(gathered[2], 1).reshape(-1, cum_gates.shape[1])
+    mixed = attend(queries, key_rows, value_rows, key_gates, cum_gates, out_proj)
+    if dense:
+        table = join_three(gathered[3], 1).reshape(-1, experts)
+        share = row_count // lax.axis_size("tp")
+        own = lax.dynamic_slice_in_dim(tokens, lax.axis_index("tp") * share, share, 0)
+        rows = lax.all_gather(normalize(own, norm_gain), ("ep", "tp"), axis=0, tiled=True)
+        routed = experts_dense(rows, table, w_gate, w_up, exchange_down(w_down[0]))
+    else:
+        routed = experts_part(
+            tokens, norm_gain, routes, route_weights, w_gate, w_up, w_down
+        )
     return (mixed, routed)
 
 

time: 320 us -> 273 us (0.85)
  blocking collectives: 151 us -> 0 us
  waiting for transfers between devices: 88 us -> 205 us
  starting transfers between devices: 13.8 us -> 3.17 us
    all_gather x3 -> x0, blocking collectives: 95.7 us -> none  [the longest x1 33.4 us: attend(): lax.all_gather(keys.astype(jnp.float32), 'ep', axis=0, tiled=True)]
    reduce_scatter x1, waiting for transfers between devices: 0.02 us -> 73.2 us  [experts_dense(): lax.psum_scatter((expert_out * mine).astype(jnp.bfloat16), 'ep', scatter_...]
    all_to_all x1 -> x0, blocking collectives: 55.4 us -> none  [experts_part(): lax.all_to_all(own_part, 'ep', split_axis=0, concat_axis=0, tiled=True)]
    all_gather x1 -> x3, waiting for transfers between devices: 57.4 us -> 110 us  [the longest x1 77 us: per_device(): lax.all_gather(normalize(own, norm_gain), ('ep', 'tp'), axis=0, tiled=True)]
    all_to_all x1 -> x0, waiting for transfers between devices: 30.5 us -> none  [experts_part(): lax.all_to_all(results, 'ep', split_axis=0, concat_axis=0, tiled=True)]
    ppermute x0 -> x3, waiting for transfers between devices: none -> 16.4 us  [exchange_down(): lax.ppermute(block, 'tp', [(i, (i + offset) % count) for i in range(count)])]
    all_to_all x1 -> x0, starting transfers between devices: 13.7 us -> none  [experts_part(): lax.all_to_all(results, 'ep', split_axis=0, concat_axis=0, tiled=True)]
    gather x2 -> x0, local copies, waits for them, and re-layouts: 12.3 us -> none  [the longest x1 7.74 us: experts_part(): normed[jnp.maximum(slot_rows, 0)]]
  transfers between devices with their start and end apart: 4 -> 8, of which waited for: 2 -> 6; matrix products, arithmetic and copies ran while one was open for 6% -> 17% of each run, Pallas kernels for 0% -> 0%
where the time goes in v1:
time: 273 us; the launch traced here: 272 us
  waiting for transfers between devices  205 us (75%)
  matrix products  22.1 us (8%)
  local copies, waits for them, and re-layouts  19.7 us (7%)
  between operations  14 us (5%)
  other arithmetic  8.3 us (3%)
  starting transfers between devices  3.17 us (1%)
    all_gather x1, waiting for transfers between devices, per_device(): lax.all_gather(normalize(own, norm_gain), ('ep', 'tp'), axis=0, tiled=True)  77 us
    reduce_scatter x1, waiting for transfers between devices, experts_dense(): lax.psum_scatter((expert_out * mine).astype(jnp.bfloat16), 'ep', scatter_...  73.2 us
    all_gather x1, waiting for transfers between devices, gather_packed(): lax.all_gather(jnp.concatenate(rows, axis=0), axis, axis=0, tiled=False)  32.6 us
    ppermute x3, waiting for transfers between devices, exchange_down(): lax.ppermute(block, 'tp', [(i, (i + offset) % count) for i in range(count)])  16.4 us
    dynamic_update_slice x4, local copies, waits for them, and re-layouts, exchange_down(): result = lax.dynamic_update_slice_in_dim(result, block, source * hidden, 0)  7.65 us
    dot_general x1, matrix products, experts_dense(): expert_out = jnp.dot(full, down, preferred_element_type=jnp.float32)  5.92 us
    dot_general x1, matrix products, experts_dense(): gate_act = jnp.dot(rows, w_gate[0], preferred_element_type=jnp.float32)  5.87 us
  transfers between devices with their start and end apart: 8, of which 6 were waited for; matrix products, arithmetic and copies ran while one was open for 17% of the time, Pallas kernels for 0%

profile of v1, /device:TPU:0, one launch (start us, length us, event | category | flops | bytes accessed | tf_op | source)
XLA Modules:
  0.0 272.1 jit_solution(7744755558400126507)
XLA Ops:
  7.2 1.2 fusion.27
  8.5 1.8 fusion.29
  10.4 0.7 select_reduce_fusion
  11.4 0.7 fusion.33
  12.6 1.5 pad_maximum_fusion
  14.2 77.0 %all-gather.5.cloned.1.call-done = bf16[1024,4096]{1,0:T(8,128)(2,1)} async-done(((bf16[32,4096]{1,0:T(8,128)(2,1)}), bf16[1024,4096]{1,0:T(8,128)(2,1)}) %all-gather.5.cloned.1.call-update) | async-done | bytes 8388624 | tf_op jit(solution)/shard_map/all_gather | solution.py:229
  91.2 5.9 %fusion.19 = f32[1024,256]{1,0:T(8,128)S(1)} fusion(bf16[1024,4096]{1,0:T(8,128)(2,1)} %all-gather.5.cloned.1.call-done, bf16[1,4096,256]{2,1,0:T(8,128)(2,1)S(1)} %copy-done), kind=kOutput, calls=%fused_computation.30 | convolution fusion | flops 2147483648 | bytes 11534336 | tf_op jit(solution)/shard_map/dot_general | solution.py:189
  97.1 0.5 copy-done.4
  97.6 3.2 %fusion.24 = bf16[1024,256]{1,0:T(8,128)(2,1)} fusion(bf16[1024,4096]{1,0:T(8,128)(2,1)S(1)} %copy-done.3, bf16[1,4096,256]{2,1,0:T(8,128)(2,1)S(1)} %copy-done.4, f32[1024,256]{1,0:T(8,128)S(1)} %fusion.19), kind=kOutput, calls=%fused_computation.33 | convolution fusion | flops 2149056512 | bytes 12058624 | tf_op jit(solution)/shard_map/dot_general | solution.py:190
  101.2 32.6 %all-gather.9.cloned.1.call-done = bf16[4608,128]{1,0:T(8,128)(2,1)} async-done(((bf16[576,128]{1,0:T(8,128)(2,1)}), bf16[4608,128]{1,0:T(8,128)(2,1)}) %all-gather.9.cloned.1.call-update) | async-done | bytes 1179664 | tf_op jit(solution)/shard_map/all_gather | solution.py:35
  133.8 0.9 slice_bitcast_fusion
  135.7 2.1 fusion.36
  138.1 2.9 %while.18 = (s32[]{:T(128)}, f32[256,1,4]{0,2,1:T(4,128)S(1)}, f32[256,1,4]{0,2,1:T(4,128)S(1)}, f32[256,1,4,128]{0,3,2,1:T(8,128)S(1)}, s32[]{:T(128)}, /*index...) while((s32[]{:T(128)}, f32[256,1,4]{0,2,1:T(4,128)S(1)}, ...), condition=%wide.region_6.7_spmd.clone, body=%wide.region_1.6_spmd.clone.sunk | while | flops 273551104 | bytes 8229221 | solution.py:104
  138.1 2.7 %conditional.3 = ((f32[256,1,4]{0,2,1:T(4,128)S(1)}, f32[256,1,4]{0,2,1:T(4,128)S(1)}, f32[256,1,4,128]{0,3,2,1:T(8,128)S(1)})) conditional(s32[]{:T(128)} %convert_element_type.87, (f32[256,1,4]{0,2,1:T(4,128)S(1)}, f32[256,1,4]{0,2,1:T(4,128)S(1)}, f32[256,1,4,128]{0,3,2,1:T(8,128)S(1)}) %tuple.61, (s32[]{:T(128)}, s32[]{:T(128)}, ...), branch_computations={%region_2.2_spmd, %region_3.5_spmd} | conditional | flops 273551104 | bytes 8227926 | solution.py:102
  138.3 1.5 fusion.35
  140.2 0.6 fusion.5
  141.1 5.0 %convolution_convert_fusion = bf16[256,4096]{1,0:T(8,128)(2,1)} fusion(bf16[256,512]{0,1:T(8,128)(2,1)S(1)} %bitcast.114, bf16[512,4096]{1,0:T(8,128)(2,1)} %param.20), kind=kOutput, calls=%fused_computation.26 | convolution fusion | flops 1074790400 | bytes 6553600 | tf_op jit(solution)/shard_map/dot_general | solution.py:111
  146.2 2.4 dynamic-slice_bitcast_fusion.1
  148.6 1.5 collective-permute-start.1
  150.1 1.5 collective-permute-start.2
  151.6 1.6 broadcast_in_dim.53
  153.2 1.9 bitcast_dynamic-update-slice_fusion
  155.1 11.2 %collective-permute-done = bf16[256,1024]{1,0:T(8,128)(2,1)} collective-permute-done((bf16[256,1024]{1,0:T(8,128)(2,1)}, bf16[256,1024]{1,0:T(8,128)(2,1)}, u32[]{:S(2)}, u32[]{:S(2)}) %collective-permute-start) | collective-permute-done | bytes 524320 | tf_op jit(solution)/shard_map/ppermute | solution.py:182
  166.3 1.9 constant_dynamic-update-slice_fusion.2
  168.3 2.0 constant_dynamic-update-slice_fusion.1
  170.2 5.2 %collective-permute-done.2 = bf16[256,1024]{1,0:T(8,128)(2,1)} collective-permute-done((bf16[256,1024]{1,0:T(8,128)(2,1)S(1)}, bf16[256,1024]{1,0:T(8,128)(2,1)}, u32[]{:S(2)}, u32[]{:S(2)}) %collective-permute-start.2) | collective-permute-done | bytes 524320 | tf_op jit(solution)/shard_map/ppermute | solution.py:182
  175.4 1.9 constant_dynamic-update-slice_fusion
  177.3 2.1 reshape.169
  179.4 1.4 slice_add_fusion
  181.2 5.9 %multiply_convert_fusion = bf16[1024,1024]{1,0:T(8,128)(2,1)} fusion(bf16[1024,1024]{1,0:T(8,128)(2,1)} %all-gather.7.cloned.1.call-done, bf16[1024,1024]{1,0:T(8,128)(2,1)} %constant_dynamic-update-slice_fusion, f32[1024]{0:T(1024)S(1)} %bitcast.121), kind=kOutput, calls=%fused_computation.27 | convolution fusion | flops 2149580800 | bytes 6295552 | tf_op jit(solution)/shard_map/dot_general | solution.py:193
  187.1 5.2 %reduce-scatter.3.cloned.1.call-done = bf16[64,4096]{1,0:T(8,128)(2,1)} async-done(((bf16[256,4096]{1,0:T(8,128)(2,1)}), bf16[64,4096]{1,0:T(8,128)(2,1)}) %reduce-scatter.3.cloned.1.call-update) | async-done | bytes 524304 | tf_op jit(solution)/shard_map/reduce_scatter | solution.py:110
  192.4 73.2 %reduce-scatter.5.cloned.1.call-done = bf16[128,1024]{1,0:T(8,128)(2,1)} async-done(((bf16[1024,1024]{1,0:T(8,128)(2,1)}), bf16[128,1024]{1,0:T(8,128)(2,1)}) %reduce-scatter.5.cloned.1.call-update) | async-done | bytes 262160 | tf_op jit(solution)/shard_map/reduce_scatter | solution.py:195
  (63 shorter events, 3.7 us)
Async XLA Ops:
  7.2 84.1 %copy-start = (bf16[1,4096,256]{2,1,0:T(8,128)(2,1)S(1)}, bf16[1,4096,256]{2,1,0:T(8,128)(2,1)}, u32[]{:S(2)}) copy-start(bf16[1,4096,256]{2,1,0:T(8,128)(2,1)} %param.25) | copy-start | bytes 6291460
  7.2 84.0 %all-gather.5.cloned.1.call-start = ((), (), s32[]{:S(2)}) async-start(), calls=%async_computation.3 | async-start | bytes 8650752 | tf_op jit(solution)/shard_map/all_gather | solution.py:229
  10.3 123.4 %all-gather.9.cloned.1.call-start = ((), (), s32[]{:S(2)}) async-start(), calls=%async_computation.6 | async-start | bytes 1327104 | tf_op jit(solution)/shard_map/all_gather | solution.py:35
  14.1 167.1 %all-gather.7.cloned.1.call-start = ((), (), s32[]{:S(2)}) async-start(), calls=%async_computation.4 | async-start | bytes 2621440 | tf_op jit(solution)/shard_map/all_gather | solution.py:192
  91.2 5.9 %copy-start.3 = (bf16[1024,4096]{1,0:T(8,128)(2,1)S(1)}, bf16[1024,4096]{1,0:T(8,128)(2,1)}, u32[]{:S(2)}) copy-start(bf16[1024,4096]{1,0:T(8,128)(2,1)} %all-gather.5.cloned.1.call-done) | copy-start | bytes 25165828
  91.2 6.4 %copy-start.4 = (bf16[1,4096,256]{2,1,0:T(8,128)(2,1)S(1)}, bf16[1,4096,256]{2,1,0:T(8,128)(2,1)}, u32[]{:S(2)}) copy-start(bf16[1,4096,256]{2,1,0:T(8,128)(2,1)} %param.26) | copy-start | bytes 6291460
  97.6 3.3 %copy-start.1 = (bf16[256,512]{1,0:T(8,128)(2,1)S(1)}, bf16[256,512]{1,0:T(8,128)(2,1)}, u32[]{:S(2)}) copy-start(bf16[256,512]{1,0:T(8,128)(2,1)} %param.16) | copy-start | bytes 786436
  100.8 91.6 %reduce-scatter.3.cloned.1.call-start = ((), (), s32[]{:S(2)}) async-start(), calls=%async_computation.2 | async-start | bytes 2621440 | tf_op jit(solution)/shard_map/reduce_scatter | solution.py:110
  135.5 2.6 copy-start.2
  146.1 119.5 %reduce-scatter.5.cloned.1.call-start = ((), (), s32[]{:S(2)}) async-start(), calls=%async_computation.5 | async-start | bytes 2359296 | tf_op jit(solution)/shard_map/reduce_scatter | solution.py:195
  148.6 17.7 %collective-permute-start = (bf16[256,1024]{1,0:T(8,128)(2,1)}, bf16[256,1024]{1,0:T(8,128)(2,1)}, u32[]{:S(2)}, u32[]{:S(2)}) collective-permute-start(bf16[256,1024]{1,0:T(8,128)(2,1)} %get-tuple-element.336), channel_id=1, source_target_pairs={{0,1},{1,2},{2,3},{3,0},{4,5},{5,6},{6,7},{7,4},{8,9},{9,10},{10,1... | collective-permute-start | bytes 1572872 | tf_op jit(solution)/shard_map/ppermute | solution.py:182
  148.6 19.6 %collective-permute-start.1 = (bf16[256,1024]{1,0:T(8,128)(2,1)S(1)}, bf16[256,1024]{1,0:T(8,128)(2,1)}, u32[]{:S(2)}, u32[]{:S(2)}) collective-permute-start(bf16[256,1024]{1,0:T(8,128)(2,1)S(1)} %get-tuple-element.337), channel_id=1, source_target_pairs={{0,2},{1,3},{2,0},{3,1},{4,6},{5,7},{6,4},{7,5},{8,10},{9,11},{10,... | collective-permute-start | bytes 1572872 | tf_op jit(solution)/shard_map/ppermute | solution.py:182
  150.1 25.3 %collective-permute-start.2 = (bf16[256,1024]{1,0:T(8,128)(2,1)S(1)}, bf16[256,1024]{1,0:T(8,128)(2,1)}, u32[]{:S(2)}, u32[]{:S(2)}) collective-permute-start(bf16[256,1024]{1,0:T(8,128)(2,1)S(1)} %get-tuple-element.335), channel_id=1, source_target_pairs={{0,3},{1,0},{2,1},{3,2},{4,7},{5,4},{6,5},{7,6},{8,11},{9,8},{10,9... | collective-permute-start | bytes 1572872 | tf_op jit(solution)/shard_map/ppermute | solution.py:182
Sparse Core Ops, SparseCore 0:
  11.4 79.7 all-gather.4
  94.0 39.7 all-gather.8
  135.3 24.8 all-gather.6
  163.2 29.1 reduce-scatter.2
  196.3 69.2 reduce-scatter.4

commit v2 on v1

--- a/solution.py
+++ b/solution.py
@@ -1,8 +1,11 @@
+import functools
 import math
 
 import jax
 import jax.numpy as jnp
 from jax import lax
+from jax.experimental import pallas as pl
+from jax.experimental.pallas import tpu as pltpu
 from jax.sharding import PartitionSpec as P
 
 HD = 128
@@ -25,14 +28,15 @@
     return (parts[2] + parts[1]) + parts[0]
 
 
-def gather_packed(arrays, axis):
+def gather_packed(arrays, axis, beside):
     lanes = 128
     rows = []
     for array in arrays:
         flat = array.reshape(-1)
         flat = jnp.pad(flat, (0, -flat.shape[0] % (16 * lanes)))
         rows.append(flat.reshape(-1, lanes))
-    gathered = lax.all_gather(jnp.concatenate(rows, axis=0), axis, axis=0, tiled=False)
+    packed, beside = lax.optimization_barrier((jnp.concatenate(rows, axis=0), beside))
+    gathered = lax.all_gather(packed, axis, axis=0, tiled=False)
     count = gathered.shape[0]
     results = []
     first = 0
@@ -42,10 +46,10 @@
             piece = piece.reshape(count, -1)[:, : array.size]
         results.append(piece.reshape((count,) + array.shape))
         first += block.shape[0]
-    return results
-
-
-def attend(queries, key_rows, value_rows, key_gates, cum_gates, out_proj):
+    return results, beside
+
+
+def attend(queries, key_rows, value_rows, key_gates, cum_gates, out_proj, beside):
     local_rows = queries.shape[0]
     groups = key_rows.shape[1] // HD
     group_ratio = cum_gates.shape[1] // groups
@@ -107,12 +111,14 @@
         .astype(jnp.bfloat16)
         .reshape(local_rows, groups * group_ratio * HD)
     )
-    return lax.psum_scatter(
+    heads_out, beside = lax.optimization_barrier((heads_out, beside))
+    mixed = lax.psum_scatter(
         jnp.dot(heads_out, out_proj, preferred_element_type=jnp.float32).astype(jnp.bfloat16),
         "tp",
         scatter_dimension=0,
         tiled=True,
     )
+    return mixed, beside
 
 
 def experts_part(tokens, norm_gain, routes, route_weights, w_gate, w_up, w_down):
@@ -185,6 +191,104 @@
     return result
 
 
+MESH = pl.DeviceIdType.MESH
+
+
+def spread_kernel(n_ep, n_tp, share, local_ref, out_ref, send_sem, recv_sem, own_sem):
+    ep = lax.axis_index("ep")
+    tp = lax.axis_index("tp")
+    near = tp + 1 - 2 * lax.rem(tp, 2)
+    far = lax.rem(tp + 2, n_tp)
+    block = share * n_tp
+
+    barrier = pltpu.get_barrier_semaphore()
+    for offset in range(1, n_ep):
+        peer = lax.rem(ep + offset, n_ep)
+        pl.semaphore_signal(barrier, inc=1, device_id=(peer, tp), device_id_type=MESH)
+    for peer in (near, far):
+        pl.semaphore_signal(barrier, inc=1, device_id=(ep, peer), device_id_type=MESH)
+    pl.semaphore_wait(barrier, n_ep + 1)
+
+    def rows(source, part):
+        return pl.ds(pl.multiple_of(source * block + part * share, share), share)
+
+    def remote(kind, offset, src, place, device):
+        return pltpu.make_async_remote_copy(
+            src_ref=src,
+            dst_ref=out_ref.at[place],
+            send_sem=send_sem.at[kind, offset - 1],
+            recv_sem=recv_sem.at[kind, offset - 1],
+            device_id=device,
+            device_id_type=MESH,
+        )
+
+    def source_of(offset):
+        return lax.rem(ep + n_ep - offset, n_ep)
+
+    def forward(kind, offset):
+        source = source_of(offset)
+        if kind == 3:
+            place = rows(source, far)
+        else:
+            place = rows(source, tp)
+        target = far if kind == 1 else near
+        return remote(kind, offset, out_ref.at[place], place, (ep, target))
+
+    mine = local_ref.at[pl.ds(pl.multiple_of(tp * share, share), share)]
+    first = []
+    for offset in range(1, n_ep):
+        peer = lax.rem(ep + offset, n_ep)
+        copy = remote(0, offset, mine, rows(ep, tp), (peer, tp))
+        copy.start()
+        first.append(copy)
+    own = pltpu.make_async_copy(
+        local_ref, out_ref.at[pl.ds(pl.multiple_of(ep * block, block), block)], own_sem
+    )
+    own.start()
+    across, beside, second = [], [], []
+    for offset in range(1, n_ep):
+        first[offset - 1].wait_recv()
+        for kind, kept in ((1, across), (2, beside)):
+            copy = forward(kind, offset)
+            copy.start()
+            kept.append(copy)
+        if offset > 1:
+            across[offset - 2].wait_recv()
+            copy = forward(3, offset - 1)
+            copy.start()
+            second.append(copy)
+    across[-1].wait_recv()
+    copy = forward(3, n_ep - 1)
+    copy.start()
+    second.append(copy)
+    for copy in beside + second:
+        copy.wait_recv()
+    own.wait()
+    for copy in first + across + beside + second:
+        copy.wait_send()
+
+
+def spread_rows(local):
+    n_ep, n_tp = lax.axis_size("ep"), lax.axis_size("tp")
+    count, features = local.shape
+    share = count // n_tp
+    sent = local.size * local.dtype.itemsize * (n_ep - 1)
+    return pl.pallas_call(
+        functools.partial(spread_kernel, n_ep, n_tp, share),
+        out_shape=jax.ShapeDtypeStruct((n_ep * count, features), local.dtype),
+        in_specs=[pl.BlockSpec(memory_space=pltpu.VMEM)],
+        out_specs=pl.BlockSpec(memory_space=pl.ANY),
+        scratch_shapes=[
+            pltpu.SemaphoreType.DMA((4, n_ep - 1)),
+            pltpu.SemaphoreType.DMA((4, n_ep - 1)),
+            pltpu.SemaphoreType.DMA,
+        ],
+        compiler_params=pltpu.CompilerParams(collective_id=0, has_side_effects=True),
+        cost_estimate=pl.CostEstimate(flops=0, bytes_accessed=12 * sent, transcendentals=0),
+        name="spread_rows",
+    )(local)
+
+
 def experts_dense(rows, table, w_gate, w_up, down):
     gate_act = jnp.dot(rows, w_gate[0], preferred_element_type=jnp.float32)
     up_act = jnp.dot(rows, w_up[0], preferred_element_type=jnp.float32)
@@ -192,9 +296,11 @@
     full = lax.all_gather(hidden, "tp", axis=1, tiled=True)
     expert_out = jnp.dot(full, down, preferred_element_type=jnp.float32)
     mine = lax.dynamic_index_in_dim(table, lax.axis_index("ep"), 1, keepdims=True)
-    return lax.psum_scatter(
-        (expert_out * mine).astype(jnp.bfloat16), "ep", scatter_dimension=0, tiled=True
-    )
+    returned = lax.all_to_all(
+        (expert_out * mine).astype(jnp.bfloat16), "ep", split_axis=0, concat_axis=0, tiled=True
+    )
+    terms = returned.reshape(lax.axis_size("ep"), -1, returned.shape[1]).astype(jnp.float32)
+    return jnp.sum(terms, axis=0).astype(jnp.bfloat16)
 
 
 def per_device(
@@ -217,18 +323,28 @@
     packed = [keys, values, split_three(cum_gates)]
     if dense:
         packed.append(split_three(combine_table(routes, route_weights, experts)))
-    gathered = gather_packed(packed, "ep")
+    tp_count = lax.axis_size("tp")
+    own = normalize(tokens, norm_gain) if dense else tokens
+    gathered, own = gather_packed(packed, "ep", own)
     key_rows = gathered[0].reshape(-1, keys.shape[1])
     value_rows = gathered[1].reshape(-1, values.shape[1])
     key_gates = join_three(gathered[2], 1).reshape(-1, cum_gates.shape[1])
-    mixed = attend(queries, key_rows, value_rows, key_gates, cum_gates, out_proj)
     if dense:
         table = join_three(gathered[3], 1).reshape(-1, experts)
-        share = row_count // lax.axis_size("tp")
-        own = lax.dynamic_slice_in_dim(tokens, lax.axis_index("tp") * share, share, 0)
-        rows = lax.all_gather(normalize(own, norm_gain), ("ep", "tp"), axis=0, tiled=True)
-        routed = experts_dense(rows, table, w_gate, w_up, exchange_down(w_down[0]))
+        if tp_count == 4 and row_count % (16 * tp_count) == 0:
+            rows = spread_rows(own)
+        else:
+            rows = lax.all_gather(own, "ep", axis=0, tiled=True)
+        rows, down_shard = lax.optimization_barrier((rows, w_down[0]))
+        down = exchange_down(down_shard)
+        mixed, down = attend(
+            queries, key_rows, value_rows, key_gates, cum_gates, out_proj, down
+        )
+        routed = experts_dense(rows, table, w_gate, w_up, down)
     else:
+        mixed, _ = attend(
+            queries, key_rows, value_rows, key_gates, cum_gates, out_proj, w_down
+        )
         routed = experts_part(
             tokens, norm_gain, routes, route_weights, w_gate, w_up, w_down
         )

time: 273 us -> 234 us (0.86)
  waiting for transfers between devices: 205 us -> 11.4 us
  blocking collectives: 0 us -> 80.9 us
  Pallas kernels: 0 us -> 73.6 us
    all_gather x2 -> x1, waiting for transfers between devices: 110 us -> 0.01 us  [gather_packed(): gathered = lax.all_gather(packed, axis, axis=0, tiled=False)]
    all_to_all x0 -> x1, blocking collectives: none -> 80.9 us  [experts_dense(): lax.all_to_all((expert_out * mine).astype(jnp.bfloat16), 'ep', split_axis...]
    pallas_call x0 -> x1, Pallas kernels: none -> 73.6 us  [spread_rows(): pl.pallas_call(functools.partial(spread_kernel, n_ep, n_tp, share), out_s...]
    reduce_scatter x1 -> x0, waiting for transfers between devices: 73.2 us -> none  [experts_dense(): lax.psum_scatter((expert_out * mine).astype(jnp.bfloat16), 'ep', scatter_...]
    ppermute x3, waiting for transfers between devices: 16.4 us -> 11 us  [exchange_down(): lax.ppermute(block, 'tp', [(i, (i + offset) % count) for i in range(count)])]
    reduce_scatter x1, waiting for transfers between devices: 5.24 us -> 0.01 us  [attend(): lax.psum_scatter(jnp.dot(heads_out, out_proj, preferred_element_type=jnp....]
    dynamic_update_slice x4 -> x3, local copies, waits for them, and re-layouts: 7.65 us -> 3.57 us  [exchange_down(): result = lax.dynamic_update_slice_in_dim(result, block, source * hidden, 0)]
    unnamed x16 -> x28, local copies, waits for them, and re-layouts: 1.93 us -> 5.81 us
  transfers between devices with their start and end apart: 8 -> 6, of which waited for: 6 -> 2; matrix products, arithmetic and copies ran while one was open for 17% -> 17% of each run, Pallas kernels for 0% -> 32%
where the time goes in v2:
time: 234 us; the launch traced here: 233 us
  blocking collectives  80.9 us (35%)
  Pallas kernels  73.6 us (31%)
  matrix products  21.5 us (9%)
  local copies, waits for them, and re-layouts  17.7 us (8%)
  between operations  14.1 us (6%)
  waiting for transfers between devices  11.4 us (5%)
  other arithmetic  10.9 us (5%)
  starting transfers between devices  2.56 us (1%)
    all_to_all x1, blocking collectives, experts_dense(): lax.all_to_all((expert_out * mine).astype(jnp.bfloat16), 'ep', split_axis...  80.9 us
    pallas_call x1, Pallas kernels, spread_rows(): pl.pallas_call(functools.partial(spread_kernel, n_ep, n_tp, share), out_s...  73.6 us
    ppermute x3, waiting for transfers between devices, exchange_down(): lax.ppermute(block, 'tp', [(i, (i + offset) % count) for i in range(count)])  11 us
    dot_general x1, matrix products, experts_dense(): gate_act = jnp.dot(rows, w_gate[0], preferred_element_type=jnp.float32)  5.95 us
    unnamed x28, local copies, waits for them, and re-layouts  5.81 us
    dot_general x1, matrix products, attend(): jnp.dot(heads_out, out_proj, preferred_element_type=jnp.float32)  4.79 us
  transfers between devices with their start and end apart: 6, of which 2 were waited for; matrix products, arithmetic and copies ran while one was open for 17% of the time, Pallas kernels for 32%

profile of v2, /device:TPU:0, one launch (start us, length us, event | category | flops | bytes accessed | tf_op | source)
XLA Modules:
  0.0 233.0 jit_solution(1451806704900150054)
XLA Ops:
  7.3 1.7 fusion.17
  8.9 0.7 select_reduce_fusion
  9.7 0.7 fusion.33
  11.2 2.1 fusion.19.local_ref
  13.3 0.7 pad_maximum_fusion
  14.1 73.6 %spread_rows.1 = bf16[1024,4096]{1,0:T(8,128)(2,1)} custom-call(bf16[128,4096]{1,0:T(8,128)(2,1)} %fusion.19.local_ref), custom_call_target="tpu_custom_call" | custom-call | bytes 88080384 | tf_op jit(solution)/shard_map/spread_rows/pallas_call | solution.py:276
  88.0 1.3 copy-done.3
  89.3 1.2 constant_dynamic-slice_fusion
  90.5 1.4 copy-done.2
  91.9 0.5 collective-permute-start
  92.4 5.9 %fusion.22 = f32[1024,256]{1,0:T(8,128)S(1)} fusion(bf16[1024,4096]{1,0:T(8,128)(2,1)} %spread_rows.1, bf16[1,4096,256]{2,1,0:T(8,128)(2,1)S(1)} %copy-done), kind=kOutput, calls=%fused_computation.35 | convolution fusion | flops 2147483648 | bytes 11534336 | tf_op jit(solution)/shard_map/dot_general | solution.py:293
  98.4 3.2 %fusion.27 = bf16[1024,256]{1,0:T(8,128)(2,1)} fusion(bf16[1024,4096]{1,0:T(8,128)(2,1)S(1)} %bitcast.101, bf16[1,4096,256]{2,1,0:T(8,128)(2,1)S(1)} %copy-done.8, f32[1024,256]{1,0:T(8,128)S(1)} %fusion.22), kind=kOutput, calls=%fused_computation.38 | convolution fusion | flops 2149056512 | bytes 12058624 | tf_op jit(solution)/shard_map/dot_general | solution.py:294
  101.6 2.0 collective-permute-start.2
  103.6 1.1 copy.51
  104.7 0.8 copy.55
  105.5 11.0 %collective-permute-done = bf16[256,1024]{1,0:T(8,128)(2,1)S(1)} collective-permute-done((bf16[256,1024]{1,0:T(8,128)(2,1)}, bf16[256,1024]{1,0:T(8,128)(2,1)S(1)}, u32[]{:S(2)}, u32[]{:S(2)}) %collective-permute-start) | collective-permute-done | bytes 524320 | tf_op jit(solution)/shard_map/ppermute | solution.py:188
  116.6 0.8 constant_dynamic-update-slice_fusion.2
  117.4 0.8 constant_dynamic-update-slice_fusion.1
  118.3 1.9 constant_dynamic-update-slice_fusion
  120.1 2.1 fusion.36
  122.3 1.0 copy.60
  123.3 0.9 slice_bitcast_fusion
  125.3 2.0 reshape.169
  127.3 1.5 slice_add_fusion
  129.2 3.9 %while.18 = (s32[]{:T(128)}, f32[256,1,4]{0,2,1:T(4,128)S(1)}, f32[256,1,4]{0,2,1:T(4,128)S(1)}, f32[256,1,4,128]{0,3,2,1:T(8,128)S(1)}, s32[]{:T(128)}, /*index...) while((s32[]{:T(128)}, f32[256,1,4]{0,2,1:T(4,128)S(1)}, ...), condition=%wide.region_7.8_spmd.clone, body=%wide.region_2.7_spmd.clone.sunk | while | flops 273551104 | bytes 8229213 | solution.py:108
  129.3 3.6 %conditional.3 = ((f32[256,1,4]{0,2,1:T(4,128)S(1)}, f32[256,1,4]{0,2,1:T(4,128)S(1)}, f32[256,1,4,128]{0,3,2,1:T(8,128)S(1)})) conditional(s32[]{:T(128)} %convert_element_type.89, (f32[256,1,4]{0,2,1:T(4,128)S(1)}, f32[256,1,4]{0,2,1:T(4,128)S(1)}, f32[256,1,4,128]{0,3,2,1:T(8,128)S(1)}) %tuple.68, (s32[]{:T(128)}, s32[]{:T(128)}, ...), branch_computations={%region_3.3_spmd, %region_4.6_spmd} | conditional | flops 273551104 | bytes 8227926 | solution.py:106
  129.5 1.6 fusion.35
  131.1 1.5 fusion.5
  133.2 4.8 %convolution_convert_fusion = bf16[256,4096]{1,0:T(8,128)(2,1)} fusion(bf16[256,512]{0,1:T(8,128)(2,1)S(1)} %bitcast.112, bf16[512,4096]{1,0:T(8,128)(2,1)} %param.20), kind=kOutput, calls=%fused_computation.26 | convolution fusion | flops 1074790400 | bytes 6553600 | tf_op jit(solution)/shard_map/dot_general | solution.py:116
  138.2 4.5 %multiply_convert_fusion = bf16[1024,1024]{1,0:T(8,128)(2,1)S(1)} fusion(bf16[1024,1024]{1,0:T(8,128)(2,1)} %all-gather.4.cloned.1.call-done, bf16[1024,1024]{1,0:T(8,128)(2,1)} %constant_dynamic-update-slice_fusion, f32[1024]{0:T(1024)S(1)} %bitcast.119), kind=kOutput, calls=%fused_computation.27 | convolution fusion | flops 2149580800 | bytes 6295552 | tf_op jit(solution)/shard_map/dot_general | solution.py:297
  142.8 80.9 %all_to_all.9 = bf16[8,128,1024]{2,1,0:T(8,128)(2,1)} all-to-all(bf16[8,128,1024]{2,1,0:T(8,128)(2,1)S(1)} %bitcast.107), channel_id=1, replica_groups=mesh['ep'=8,'tp'=4] {'ep'}, dimensions={0} | all-to-all | bytes 4194304 | tf_op jit(solution)/shard_map/all_to_all | solution.py:299
  223.8 2.7 %reduce_sum.46 = bf16[128,1024]{1,0:T(8,128)(2,1)} reduce(bf16[8,128,1024]{2,1,0:T(8,128)(2,1)} %all_to_all.9, bf16[]{:T(256)} %constant.105.clone.1), dimensions={0}, to_apply=%region_9.10 | reduce | flops 917504 | bytes 2359298 | tf_op jit(solution)/shard_map/reduce_sum | solution.py:303
  (72 shorter events, 3.6 us)
Async XLA Ops:
  7.2 85.3 %copy-start = (bf16[1,4096,256]{2,1,0:T(8,128)(2,1)S(1)}, bf16[1,4096,256]{2,1,0:T(8,128)(2,1)}, u32[]{:S(2)}) copy-start(bf16[1,4096,256]{2,1,0:T(8,128)(2,1)} %param.25) | copy-start | bytes 6291460
  7.2 4.0 %copy-start.1 = (bf16[128,4096]{1,0:T(8,128)(2,1)S(1)}, bf16[128,4096]{1,0:T(8,128)(2,1)}, u32[]{:S(2)}) copy-start(bf16[128,4096]{1,0:T(8,128)(2,1)} %param.21) | copy-start | bytes 3145732
  7.2 6.1 %copy-start.5 = (bf16[256,128]{1,0:T(8,128)(2,1)S(1)}, bf16[256,128]{1,0:T(8,128)(2,1)}, u32[]{:S(2)}) copy-start(bf16[256,128]{1,0:T(8,128)(2,1)} %param.18) | copy-start | bytes 196612
  7.2 6.1 %copy-start.6 = (bf16[256,128]{1,0:T(8,128)(2,1)S(1)}, bf16[256,128]{1,0:T(8,128)(2,1)}, u32[]{:S(2)}) copy-start(bf16[256,128]{1,0:T(8,128)(2,1)} %param.17) | copy-start | bytes 196612
  7.2 112.9 %all-gather.6.cloned.1.call-start = ((), (), s32[]{:S(2)}) async-start(), calls=%async_computation.4 | async-start | bytes 1327104 | tf_op jit(solution)/shard_map/all_gather | solution.py:39
  14.0 124.3 %all-gather.4.cloned.1.call-start = ((), (), s32[]{:S(2)}) async-start(), calls=%async_computation.3 | async-start | bytes 2621440 | tf_op jit(solution)/shard_map/all_gather | solution.py:296
  87.7 1.6 copy-start.3
  90.5 1.4 copy-start.2
  91.9 25.5 %collective-permute-start.1 = (bf16[256,1024]{1,0:T(8,128)(2,1)}, bf16[256,1024]{1,0:T(8,128)(2,1)S(1)}, u32[]{:S(2)}, u32[]{:S(2)}) collective-permute-start(bf16[256,1024]{1,0:T(8,128)(2,1)} %get-tuple-element.348), channel_id=1, source_target_pairs={{0,2},{1,3},{2,0},{3,1},{4,6},{5,7},{6,4},{7,5},{8,10},{9,11},{10,... | collective-permute-start | bytes 1572872 | tf_op jit(solution)/shard_map/ppermute | solution.py:188
  91.9 6.4 %slice-start = ((s8[8388608]{0:T(1024)(128)(4,1)}), s8[4194304]{0:T(1024)(128)(4,1)S(1)}, s32[]{:S(2)}) async-start(s8[8388608]{0:T(1024)(128)(4,1)} %bitcast.100), calls=%async_computation.5 | async-start | bytes 8388608
  91.9 6.4 %slice-start.1 = ((s8[8388608]{0:T(1024)(128)(4,1)}), s8[4194304]{0:T(1024)(128)(4,1)S(1)}, s32[]{:S(2)}) async-start(s8[8388608]{0:T(1024)(128)(4,1)} %bitcast.100), calls=%async_computation.6 | async-start | bytes 8388608
  91.9 6.5 %copy-start.8 = (bf16[1,4096,256]{2,1,0:T(8,128)(2,1)S(1)}, bf16[1,4096,256]{2,1,0:T(8,128)(2,1)}, u32[]{:S(2)}) copy-start(bf16[1,4096,256]{2,1,0:T(8,128)(2,1)} %param.26) | copy-start | bytes 6291460
  91.9 24.6 %collective-permute-start = (bf16[256,1024]{1,0:T(8,128)(2,1)}, bf16[256,1024]{1,0:T(8,128)(2,1)S(1)}, u32[]{:S(2)}, u32[]{:S(2)}) collective-permute-start(bf16[256,1024]{1,0:T(8,128)(2,1)} %get-tuple-element.349), channel_id=1, source_target_pairs={{0,1},{1,2},{2,3},{3,0},{4,5},{5,6},{6,7},{7,4},{8,9},{9,10},{10,1... | collective-permute-start | bytes 1572872 | tf_op jit(solution)/shard_map/ppermute | solution.py:188
  101.6 124.9 %reduce-scatter.2.cloned.1.call-start = ((), (), s32[]{:S(2)}) async-start(), calls=%async_computation.2 | async-start | bytes 2621440 | tf_op jit(solution)/shard_map/reduce_scatter | solution.py:115
  101.6 16.6 %collective-permute-start.2 = (bf16[256,1024]{1,0:T(8,128)(2,1)}, bf16[256,1024]{1,0:T(8,128)(2,1)}, u32[]{:S(2)}, u32[]{:S(2)}) collective-permute-start(bf16[256,1024]{1,0:T(8,128)(2,1)} %get-tuple-element.347), channel_id=1, source_target_pairs={{0,3},{1,0},{2,1},{3,2},{4,7},{5,4},{6,5},{7,6},{8,11},{9,8},{10,9... | collective-permute-start | bytes 1572872 | tf_op jit(solution)/shard_map/ppermute | solution.py:188
  127.3 1.9 copy-start.4
  127.3 1.9 copy-start.7
Sparse Core Ops, SparseCore 0:
  14.1 68.6 all-gather.5
  101.7 36.4 all-gather.3
  141.4 55.0 reduce-scatter.1
